TPU v7x, 32 devices: a whole 2x2x4 slice. The times are simulated.
32 devices in a mesh: sp: 8 (over z, y), tp: 4 (over x, core).
Axes of the slice: x: 2, y: 2, z: 4, core: 2. Of those that a mesh axis runs over, the one named last changes fastest.
Arguments:
- tokens_in: bfloat16 [2048, 2048], P('sp'), may hold values from -3 to 3
- queries: bfloat16 [2048, 1024], P('sp', 'tp'), may hold values from -6 to 6
- keys: bfloat16 [2048, 256], P('sp', 'tp'), may hold values from -6 to 6
- values: bfloat16 [2048, 256], P('sp', 'tp'), may hold values from -12 to 12
- doc_ids: int32 [2048], P('sp'), may hold values from 0 to 1, never falling along the last dimension, each value on 1 to 1280 neighbouring positions
- query_gain: float32 [64], replicated, may hold values from 2.5 to 6
- key_norm_scale: float32 [64], replicated, may hold values from 2.5 to 6
- out_weight: bfloat16 [1024, 2048], P('tp'), may hold values from -0.1875 to 0.1875
- norm_gain: float32 [2048], replicated, may hold values from 0.1 to 1.9
- gate_weight: bfloat16 [2048, 5632], P('sp', 'tp'), may hold values from -0.125 to 0.125
- up_weight: bfloat16 [2048, 5632], P('sp', 'tp'), may hold values from -0.125 to 0.125
- down_weight: bfloat16 [5632, 2048], P('tp', 'sp'), may hold values from -0.078125 to 0.078125
Outputs:
- layer_out: bfloat16 [2048, 2048], P('sp')
Inputs may be any that keep to these rules, and one draw needn't show every extreme that they name: `doc_ids`: document numbers never fall along the sequence; every document has 1 to 1280 positions and one has exactly 1280.
All inputs are finite; a program needn't handle non-finite values.
Results may differ from a plain program's by a relative error of at most 0.014.
The roundings to bfloat16 on the way count: a program that leaves them out, or rounds other values in their place, can miss the bound.
Values may be sent and summed in bfloat16 or wider, within the bound.
A program may use at most 128 MiB of HBM per device.

v0:
```python
import jax
import jax.numpy as jnp
from jax import lax
from jax.sharding import PartitionSpec as P

GRID = 64
EPS = 1e-06
THETA = 10000.0
NEG = -1e30


def rotate_half(block, angle):
    half_dim = block.shape[-1] // 2
    cosine = jnp.cos(angle)[:, None, :]
    sine = jnp.sin(angle)[:, None, :]
    first = block[..., :half_dim]
    second = block[..., half_dim:]
    return jnp.concatenate(
        [first * cosine - second * sine, second * cosine + first * sine], axis=-1
    )


def normalized_rotated(values_in, gain, heads, lattice_row, lattice_column):
    full = values_in.astype(jnp.float32).reshape(values_in.shape[0], heads, -1)
    full = full * lax.rsqrt(jnp.mean(full * full, axis=-1, keepdims=True) + EPS) * gain
    half_dim = full.shape[-1] // 2
    freqs = THETA ** (-2.0 * jnp.arange(half_dim // 2, dtype=jnp.float32) / half_dim)
    by_row = rotate_half(full[..., :half_dim], lattice_row[:, None] * freqs[None, :])
    by_col = rotate_half(full[..., half_dim:], lattice_column[:, None] * freqs[None, :])
    return jnp.concatenate([by_row, by_col], axis=-1).astype(jnp.bfloat16)


def per_device(
    tokens_in,
    queries,
    keys,
    values,
    doc_ids,
    query_gain,
    key_norm_scale,
    out_weight,
    norm_gain,
    gate_weight,
    up_weight,
    down_weight,
):
    tok_rows = tokens_in.shape[0]
    head_dim = query_gain.shape[0]
    local_heads = queries.shape[1] // head_dim
    places = lax.axis_index("sp") * tok_rows + jnp.arange(tok_rows, dtype=jnp.int32)
    lattice_row = (places // GRID).astype(jnp.float32)
    lattice_column = (places % GRID).astype(jnp.float32)
    q_local = normalized_rotated(queries, query_gain, local_heads, lattice_row, lattice_column)
    q_rows = q_local.transpose(1, 0, 2).reshape(local_heads * tok_rows, head_dim)
    key_pairs = normalized_rotated(keys, key_norm_scale, 1, lattice_row, lattice_column).reshape(
        tok_rows // 2, 2 * head_dim
    )
    value_pairs = values.reshape(tok_rows // 2, 2 * head_dim)
    doc_pairs = doc_ids.reshape(tok_rows // 2, 2)
    row_docs = jnp.tile(doc_ids, local_heads)
    first_doc = doc_ids[0]
    last_doc = doc_ids[-1]
    scale = head_dim ** (-0.5)
    total_rows = local_heads * tok_rows

    def absorb_block(state, key_block, value_block, doc_block):

        def absorb(current):
            running_max, running_sum, running_acc = current
            scores = (
                jnp.einsum("qd,kd->qk", q_rows, key_block, preferred_element_type=jnp.float32)
                * scale
            )
            same = row_docs[:, None] == doc_block[None, :]
            scores = jnp.where(same, scores, NEG)
            new_max = jnp.maximum(running_max, jnp.max(scores, axis=1))
            weights = jnp.where(same, jnp.exp(scores - new_max[:, None]), 0.0)
            shrink = jnp.exp(running_max - new_max)
            new_sum = running_sum * shrink + jnp.sum(weights, axis=1)
            new_acc = running_acc * shrink[:, None] + jnp.dot(
                weights.astype(jnp.bfloat16), value_block, preferred_element_type=jnp.float32
            )
            return (new_max, new_sum, new_acc)

        touches = (doc_block[0] <= last_doc) & (doc_block[-1] >= first_doc)
        return lax.cond(touches, absorb, lambda current: current, state)

    initial = (
        jnp.full((total_rows,), NEG, jnp.float32),
        jnp.zeros((total_rows,), jnp.float32),
        jnp.zeros((total_rows, head_dim), jnp.float32),
    )
    carry = initial
    key_piece = lax.all_gather(key_pairs, "sp", axis=0, tiled=True)
    value_piece = lax.all_gather(value_pairs, "sp", axis=0, tiled=True)
    doc_piece = lax.all_gather(doc_pairs, "sp", axis=0, tiled=True)
    shards = key_piece.shape[0] * 2 // tok_rows
    joined = 1
    while joined * 2 <= shards and shards % (joined * 2) == 0 and (joined * 2 * tok_rows <= 1024):
        joined = joined * 2
    blocks = shards // joined
    span_rows = joined * tok_rows
    key_blocks = key_piece.reshape(blocks, span_rows, head_dim)
    value_blocks = value_piece.reshape(blocks, span_rows, head_dim)
    doc_blocks = doc_piece.reshape(blocks, span_rows)

    def visit(state, inputs):
        key_block, value_block, doc_block = inputs
        return (absorb_block(state, key_block, value_block, doc_block), None)

    carry, unused = lax.scan(visit, carry, (key_blocks, value_blocks, doc_blocks))
    attended = (carry[2] / carry[1][:, None]).astype(jnp.bfloat16)
    attended = (
        attended.reshape(local_heads, tok_rows, head_dim)
        .transpose(1, 0, 2)
        .reshape(tok_rows, local_heads * head_dim)
    )
    partial_value = jnp.dot(attended, out_weight, preferred_element_type=jnp.float32)
    mixed = lax.psum(
        partial_value.astype(jnp.bfloat16).astype(jnp.float32).astype(jnp.bfloat16), "tp"
    ).astype(jnp.float32)
    resid = tokens_in.astype(jnp.float32) + mixed
    normed = (
        resid * lax.rsqrt(jnp.mean(resid * resid, axis=-1, keepdims=True) + EPS) * norm_gain
    ).astype(jnp.bfloat16)
    gate = jnp.dot(
        normed,
        lax.all_gather(gate_weight, "sp", axis=0, tiled=True),
        preferred_element_type=jnp.float32,
    )
    up_val = jnp.dot(
        normed,
        lax.all_gather(up_weight, "sp", axis=0, tiled=True),
        preferred_element_type=jnp.float32,
    )
    hidden = (jax.nn.silu(gate) * up_val).astype(jnp.bfloat16)
    fed_part = jnp.dot(
        hidden,
        lax.all_gather(down_weight, "sp", axis=1, tiled=True),
        preferred_element_type=jnp.float32,
    )
    fed = lax.psum(
        fed_part.astype(jnp.bfloat16).astype(jnp.float32).astype(jnp.bfloat16), "tp"
    ).astype(jnp.float32)
    return (resid + fed).astype(jnp.bfloat16)


def solution(mesh):
    return jax.shard_map(
        per_device,
        mesh=mesh,
        in_specs=(
            P("sp", None),
            P("sp", "tp"),
            P("sp", "tp"),
            P("sp", "tp"),
            P("sp"),
            P(),
            P(),
            P("tp", None),
            P(),
            P("sp", "tp"),
            P("sp", "tp"),
            P("tp", "sp"),
        ),
        out_specs=P("sp", None),
        check_vma=False,
    )
```

profile of v0, /device:TPU:0, one launch (start us, length us, event | category | flops | bytes accessed | tf_op | source)
XLA Modules:
  0.0 460.8 jit_solution(11020853297494062564)
XLA Ops:
  7.4 1.4 fusion.48
  8.8 0.8 reshape.319
  9.6 1.0 copy.18
  10.7 0.7 fusion.22
  11.9 0.8 fusion.23
  12.7 0.8 fusion.25
  14.0 32.6 %all_gather.19 = bf16[1024,128]{1,0:T(8,128)(2,1)S(1)} all-gather(bf16[128,128]{1,0:T(8,128)(2,1)S(1)} %convert_element_type.69), channel_id=1, replica_groups=mesh['sp'=8,'tp'=4] {'sp'}, dimensions={0}, use_global_device_ids=true | all-gather | bytes 294912 | tf_op jit(solution)/shard_map/all_gather | solution.py:94
  46.5 0.2 reshape.321
  46.8 0.9 copy.20
  47.7 30.7 %all_gather.20 = bf16[1024,128]{1,0:T(8,128)(2,1)S(1)} all-gather(bf16[128,128]{1,0:T(8,128)(2,1)S(1)} %reshape.325), channel_id=1, replica_groups=mesh['sp'=8,'tp'=4] {'sp'}, dimensions={0}, use_global_device_ids=true | all-gather | bytes 294912 | tf_op jit(solution)/shard_map/all_gather | solution.py:95
  78.7 31.2 %all_gather.18 = s32[1024,2]{1,0:T(8,128)S(1)} all-gather(s32[128,2]{1,0:T(8,128)S(1)} %reshape.319), channel_id=1, replica_groups=mesh['sp'=8,'tp'=4] {'sp'}, dimensions={0}, use_global_device_ids=true | all-gather | bytes 9216 | tf_op jit(solution)/shard_map/all_gather | solution.py:96
  109.9 0.3 reshape.320
  110.3 9.8 %while.15 = (s32[]{:T(128)}, f32[1024]{0:T(1024)S(1)}, f32[1024]{0:T(1024)S(1)}, f32[1024,64]{0,1:T(8,128)S(1)}, s32[2,1024]{1,0:T(2,128)S(1)}, /*index=5*/s32[]...) while((s32[]{:T(128)}, f32[1024]{0:T(1024)S(1)}, ...), condition=%wide.region_7.8_spmd.clone, body=%wide.region_2.7_spmd.clone.sunk | while | flops 285345792 | bytes 14005583 | solution.py:111
  110.3 0.6 fusion.56
  113.4 3.6 conditional.3
  113.4 0.7 fusion.2
  114.2 1.5 fusion.4
  115.7 1.2 fusion.7
  117.0 0.6 fusion.56
  120.3 1.4 convolution_convert_fusion
  121.8 0.5 all-gather.4.cloned.1.call-update
  122.3 0.5 all-gather.6.cloned.1.call-update
  122.9 0.5 all-gather.8.cloned.1.call-update
  123.5 39.6 %all-reduce.3.cloned.1.call-done = bf16[256,2048]{1,0:T(8,128)(2,1)} async-done(((bf16[256,2048]{1,0:T(8,128)(2,1)}), bf16[256,2048]{1,0:T(8,128)(2,1)}) %all-reduce.3.cloned.1.call-update) | async-done | bytes 1048592 | tf_op jit(solution)/shard_map/psum | solution.py:119
  163.1 1.7 multiply_reduce_fusion
  164.8 56.4 %all-gather.4.cloned.1.call-done = bf16[2048,1408]{1,0:T(8,128)(2,1)} async-done(((bf16[256,1408]{1,0:T(8,128)(2,1)}), bf16[2048,1408]{1,0:T(8,128)(2,1)}) %all-gather.4.cloned.1.call-update) | async-done | bytes 5767184 | tf_op jit(solution)/shard_map/all_gather | solution.py:128
  221.2 6.0 %fusion.46 = f32[256,1408]{1,0:T(8,128)} fusion(bf16[2048,1408]{1,0:T(8,128)(2,1)} %all-gather.4.cloned.1.call-done, bf16[256,2048]{1,0:T(8,128)(2,1)} %all-reduce.3.cloned.1.call-done, bf16[256,2048]{1,0:T(8,128)(2,1)S(1)} %copy-done.1, f32[2048]{0:T(1024)S(1)} %copy-done.4, f32[256]{0:T(256)S(1)} %add_rsqrt_fusion.1), kind=kOutput, calls=%fused_computation.86 | convolution fusion | flops 1479540736 | bytes 9315328 | tf_op jit(solution)/shard_map/dot_general | solution.py:126
  227.2 86.3 %all-gather.6.cloned.1.call-done = bf16[2048,1408]{1,0:T(8,128)(2,1)} async-done(((bf16[256,1408]{1,0:T(8,128)(2,1)}), bf16[2048,1408]{1,0:T(8,128)(2,1)}) %all-gather.6.cloned.1.call-update) | async-done | bytes 5767184 | tf_op jit(solution)/shard_map/all_gather | solution.py:133
  313.6 93.0 %all-gather.8.cloned.1.call-done = bf16[1408,2048]{1,0:T(8,128)(2,1)} async-done(((bf16[1408,256]{1,0:T(8,128)(2,1)}), bf16[1408,2048]{1,0:T(8,128)(2,1)}) %all-gather.8.cloned.1.call-update) | async-done | bytes 5767184 | tf_op jit(solution)/shard_map/all_gather | solution.py:139
  406.5 9.3 %convolution_convert_fusion.1 = bf16[256,2048]{1,0:T(8,128)(2,1)} fusion(bf16[1408,2048]{1,0:T(8,128)(2,1)} %all-gather.8.cloned.1.call-done, bf16[2048,1408]{1,0:T(8,128)(2,1)} %all-gather.6.cloned.1.call-done, f32[256,1408]{1,0:T(8,128)} %fusion.46, bf16[256,2048]{1,0:T(8,128)(2,1)S(1)} %copy-done.2, bf16[256,2048]{1,0:T(8,128)(2,1)S(1)} %copy-done.1, ...), kind=kOutput, calls=%fused_computation.26 | convolution fusion | flops 2958622720 | bytes 16131072 | tf_op jit(solution)/shard_map/dot_general | solution.py:137
  415.8 34.6 %all-reduce.5.cloned.1.call-done = bf16[256,2048]{1,0:T(8,128)(2,1)} async-done(((bf16[256,2048]{1,0:T(8,128)(2,1)}), bf16[256,2048]{1,0:T(8,128)(2,1)}) %all-reduce.5.cloned.1.call-update) | async-done | bytes 1048592 | tf_op jit(solution)/shard_map/psum | solution.py:142
  450.5 2.7 add_convert_fusion
  (47 shorter events, 1.7 us)
Async XLA Ops:
  7.4 112.9 %copy-start = (bf16[256,2048]{1,0:T(8,128)(2,1)S(1)}, bf16[256,2048]{1,0:T(8,128)(2,1)}, u32[]{:S(2)}) copy-start(bf16[256,2048]{1,0:T(8,128)(2,1)} %param.23) | copy-start | bytes 3145732
  7.4 102.9 %copy-start.3 = (s32[256]{0:T(256)S(1)}, s32[256]{0:T(256)}, u32[]{:S(2)}) copy-start(s32[256]{0:T(256)} %param.20) | copy-start | bytes 3076
  7.4 155.7 %all-reduce.3.cloned.1.call-start = ((), (), s32[]{:S(2)}) async-start(), calls=%async_computation | async-start | bytes 2097152 | tf_op jit(solution)/shard_map/psum | solution.py:119
  120.1 43.0 %copy-start.1 = (bf16[256,2048]{1,0:T(8,128)(2,1)S(1)}, bf16[256,2048]{1,0:T(8,128)(2,1)}, u32[]{:S(2)}) copy-start(bf16[256,2048]{1,0:T(8,128)(2,1)} %param.16) | copy-start | bytes 3145732
  120.1 101.1 %copy-start.4 = (f32[2048]{0:T(1024)S(1)}, f32[2048]{0:T(1024)}, u32[]{:S(2)}) copy-start(f32[2048]{0:T(1024)} %param.24) | copy-start | bytes 24580
  121.7 99.5 %all-gather.4.cloned.1.call-start = ((), (), s32[]{:S(2)}) async-start(), calls=%async_computation.1 | async-start | bytes 6488064 | tf_op jit(solution)/shard_map/all_gather | solution.py:128
  122.3 191.3 %all-gather.6.cloned.1.call-start = ((), (), s32[]{:S(2)}) async-start(), calls=%async_computation.2 | async-start | bytes 6488064 | tf_op jit(solution)/shard_map/all_gather | solution.py:133
  122.9 283.6 %all-gather.8.cloned.1.call-start = ((), (), s32[]{:S(2)}) async-start(), calls=%async_computation.3 | async-start | bytes 6488064 | tf_op jit(solution)/shard_map/all_gather | solution.py:139
  123.5 327.0 %all-reduce.5.cloned.1.call-start = ((), (), s32[]{:S(2)}) async-start(), calls=%async_computation.4 | async-start | bytes 2097152 | tf_op jit(solution)/shard_map/psum | solution.py:142
  164.8 241.8 %copy-start.2 = (bf16[256,2048]{1,0:T(8,128)(2,1)S(1)}, bf16[256,2048]{1,0:T(8,128)(2,1)}, u32[]{:S(2)}) copy-start(bf16[256,2048]{1,0:T(8,128)(2,1)} %all-reduce.3.cloned.1.call-done) | copy-start | bytes 3145732
Sparse Core Ops, SparseCore 0:
  121.8 41.1 all-reduce.2
  415.9 34.4 all-reduce.4
Sparse Core Ops, SparseCore 1:
  124.4 96.8 all-gather.3
  223.3 90.2 all-gather.5
  315.5 91.0 all-gather.7
where the time goes:
time: 461 us
  waiting for transfers between devices  312 us (68%)
  blocking collectives  94.5 us (20%)
  matrix products  18.7 us (4%)
  between operations  15.2 us (3%)
  other arithmetic  8.87 us (2%)
  local copies, waits for them, and re-layouts  6.72 us (1%)
  loops' own time  5.06 us (1%)
    all_gather x1, waiting for transfers between devices, per_device(): lax.all_gather(down_weight, 'sp', axis=1, tiled=True)  93 us
    all_gather x1, waiting for transfers between devices, per_device(): lax.all_gather(up_weight, 'sp', axis=0, tiled=True)  86.3 us
    all_gather x1, waiting for transfers between devices, per_device(): lax.all_gather(gate_weight, 'sp', axis=0, tiled=True)  56.4 us
    psum x1, waiting for transfers between devices, per_device(): lax.psum(partial_value.astype(jnp.bfloat16).astype(jnp.float32).astype(jn...  39.6 us
    psum x1, waiting for transfers between devices, per_device(): lax.psum(fed_part.astype(jnp.bfloat16).astype(jnp.float32).astype(jnp.bfl...  34.6 us
    all_gather x1, blocking collectives, per_device(): key_piece = lax.all_gather(key_pairs, 'sp', axis=0, tiled=True)  32.6 us
    all_gather x1, blocking collectives, per_device(): doc_piece = lax.all_gather(doc_pairs, 'sp', axis=0, tiled=True)  31.2 us
    all_gather x1, blocking collectives, per_device(): value_piece = lax.all_gather(value_pairs, 'sp', axis=0, tiled=True)  30.7 us
  transfers between devices with their start and end apart: 5, of which 5 were waited for; matrix products, arithmetic and copies ran while one was open for 2% of the time, Pallas kernels for 0%

commit v1 on v0

--- a/solution.py
+++ b/solution.py
@@ -139,8 +139,11 @@
         lax.all_gather(down_weight, "sp", axis=1, tiled=True),
         preferred_element_type=jnp.float32,
     )
-    fed = lax.psum(
-        fed_part.astype(jnp.bfloat16).astype(jnp.float32).astype(jnp.bfloat16), "tp"
+    fed = jnp.sum(
+        lax.all_gather(
+            fed_part.astype(jnp.bfloat16).astype(jnp.float32).astype(jnp.bfloat16), "tp"
+        ),
+        axis=0,
     ).astype(jnp.float32)
     return (resid + fed).astype(jnp.bfloat16)
 

time: 461 us -> 464 us (level)
    psum x1 -> x0, waiting for transfers between devices: 34.6 us -> none  [per_device(): lax.psum(fed_part.astype(jnp.bfloat16).astype(jnp.float32).astype(jnp.bfl...]
    all_gather x0 -> x1, waiting for transfers between devices: none -> 32.7 us  [per_device(): lax.all_gather(fed_part.astype(jnp.bfloat16).astype(jnp.float32).astype(j...]
    all_gather x1, waiting for transfers between devices: 86.3 us -> 92.4 us  [per_device(): lax.all_gather(up_weight, 'sp', axis=0, tiled=True)]
    all_gather x1, waiting for transfers between devices: 93 us -> 87 us  [per_device(): lax.all_gather(down_weight, 'sp', axis=1, tiled=True)]
where the time goes in v1:
time: 464 us; the launch traced here: 463 us
  waiting for transfers between devices  310 us (67%)
  blocking collectives  94.5 us (20%)
  matrix products  18.6 us (4%)
  between operations  15.2 us (3%)
  other arithmetic  13.1 us (3%)
  local copies, waits for them, and re-layouts  6.74 us (1%)
  loops' own time  5.06 us (1%)
    all_gather x1, waiting for transfers between devices, per_device(): lax.all_gather(up_weight, 'sp', axis=0, tiled=True)  92.4 us
    all_gather x1, waiting for transfers between devices, per_device(): lax.all_gather(down_weight, 'sp', axis=1, tiled=True)  87 us
    all_gather x1, waiting for transfers between devices, per_device(): lax.all_gather(gate_weight, 'sp', axis=0, tiled=True)  56.4 us
    psum x1, waiting for transfers between devices, per_device(): lax.psum(partial_value.astype(jnp.bfloat16).astype(jnp.float32).astype(jn...  39.4 us
    all_gather x1, waiting for transfers between devices, per_device(): lax.all_gather(fed_part.astype(jnp.bfloat16).astype(jnp.float32).astype(j...  32.7 us
    all_gather x1, blocking collectives, per_device(): key_piece = lax.all_gather(key_pairs, 'sp', axis=0, tiled=True)  32.6 us
    all_gather x1, blocking collectives, per_device(): doc_piece = lax.all_gather(doc_pairs, 'sp', axis=0, tiled=True)  31.2 us
    all_gather x1, blocking collectives, per_device(): value_piece = lax.all_gather(value_pairs, 'sp', axis=0, tiled=True)  30.7 us
  transfers between devices with their start and end apart: 5, of which 5 were waited for; matrix products, arithmetic and copies ran while one was open for 2% of the time, Pallas kernels for 0%

profile of v1, /device:TPU:0, one launch (start us, length us, event | category | flops | bytes accessed | tf_op | source)
XLA Modules:
  0.0 463.2 jit_solution(11402604148512855925)
XLA Ops:
  7.4 1.4 fusion.48
  8.8 0.8 reshape.319
  9.6 1.0 copy.18
  10.7 0.7 fusion.22
  11.9 0.8 fusion.23
  12.7 0.8 fusion.25
  14.0 32.6 %all_gather.25 = bf16[1024,128]{1,0:T(8,128)(2,1)S(1)} all-gather(bf16[128,128]{1,0:T(8,128)(2,1)S(1)} %convert_element_type.71), channel_id=1, replica_groups=mesh['sp'=8,'tp'=4] {'sp'}, dimensions={0}, use_global_device_ids=true | all-gather | bytes 294912 | tf_op jit(solution)/shard_map/all_gather | solution.py:94
  46.8 0.9 copy.20
  47.8 30.7 %all_gather.26 = bf16[1024,128]{1,0:T(8,128)(2,1)S(1)} all-gather(bf16[128,128]{1,0:T(8,128)(2,1)S(1)} %reshape.325), channel_id=1, replica_groups=mesh['sp'=8,'tp'=4] {'sp'}, dimensions={0}, use_global_device_ids=true | all-gather | bytes 294912 | tf_op jit(solution)/shard_map/all_gather | solution.py:95
  78.8 31.2 %all_gather.24 = s32[1024,2]{1,0:T(8,128)S(1)} all-gather(s32[128,2]{1,0:T(8,128)S(1)} %reshape.319), channel_id=1, replica_groups=mesh['sp'=8,'tp'=4] {'sp'}, dimensions={0}, use_global_device_ids=true | all-gather | bytes 9216 | tf_op jit(solution)/shard_map/all_gather | solution.py:96
  110.0 0.3 reshape.320
  110.3 9.8 %while.15 = (s32[]{:T(128)}, f32[1024]{0:T(1024)S(1)}, f32[1024]{0:T(1024)S(1)}, f32[1024,64]{0,1:T(8,128)S(1)}, s32[2,1024]{1,0:T(2,128)S(1)}, /*index=5*/s32[]...) while((s32[]{:T(128)}, f32[1024]{0:T(1024)S(1)}, ...), condition=%wide.region_7.8_spmd.clone, body=%wide.region_2.7_spmd.clone.sunk | while | flops 285345792 | bytes 14005583 | solution.py:111
  110.4 0.6 fusion.56
  113.4 3.6 conditional.3
  113.4 0.7 fusion.2
  114.2 1.5 fusion.4
  115.8 1.2 fusion.7
  117.0 0.6 fusion.56
  120.3 1.4 convolution_convert_fusion
  121.8 0.5 all-gather.6.cloned.1.call-update
  122.4 0.5 all-gather.10.cloned.1.call-update
  123.0 0.5 all-gather.8.cloned.1.call-update
  123.7 39.4 %all-reduce.2.cloned.1.call-done = bf16[256,2048]{1,0:T(8,128)(2,1)} async-done(((bf16[256,2048]{1,0:T(8,128)(2,1)}), bf16[256,2048]{1,0:T(8,128)(2,1)}) %all-reduce.2.cloned.1.call-update) | async-done | bytes 1048592 | tf_op jit(solution)/shard_map/psum | solution.py:119
  163.1 1.6 multiply_reduce_fusion
  164.8 56.4 %all-gather.6.cloned.1.call-done = bf16[2048,1408]{1,0:T(8,128)(2,1)} async-done(((bf16[256,1408]{1,0:T(8,128)(2,1)}), bf16[2048,1408]{1,0:T(8,128)(2,1)}) %all-gather.6.cloned.1.call-update) | async-done | bytes 5767184 | tf_op jit(solution)/shard_map/all_gather | solution.py:128
  221.2 6.0 %fusion.46 = f32[256,1408]{1,0:T(8,128)} fusion(bf16[2048,1408]{1,0:T(8,128)(2,1)} %all-gather.6.cloned.1.call-done, bf16[256,2048]{1,0:T(8,128)(2,1)} %all-reduce.2.cloned.1.call-done, bf16[256,2048]{1,0:T(8,128)(2,1)S(1)} %copy-done.1, f32[2048]{0:T(1024)S(1)} %copy-done.4, f32[256]{0:T(256)S(1)} %add_rsqrt_fusion.1), kind=kOutput, calls=%fused_computation.86 | convolution fusion | flops 1479540736 | bytes 9315328 | tf_op jit(solution)/shard_map/dot_general | solution.py:126
  227.2 87.0 %all-gather.10.cloned.1.call-done = bf16[1408,2048]{1,0:T(8,128)(2,1)} async-done(((bf16[1408,256]{1,0:T(8,128)(2,1)}), bf16[1408,2048]{1,0:T(8,128)(2,1)}) %all-gather.10.cloned.1.call-update) | async-done | bytes 5767184 | tf_op jit(solution)/shard_map/all_gather | solution.py:139
  314.2 92.4 %all-gather.8.cloned.1.call-done = bf16[2048,1408]{1,0:T(8,128)(2,1)} async-done(((bf16[256,1408]{1,0:T(8,128)(2,1)}), bf16[2048,1408]{1,0:T(8,128)(2,1)}) %all-gather.8.cloned.1.call-update) | async-done | bytes 5767184 | tf_op jit(solution)/shard_map/all_gather | solution.py:133
  406.6 9.2 %convolution_convert_fusion.1 = bf16[256,2048]{1,0:T(8,128)(2,1)} fusion(bf16[1408,2048]{1,0:T(8,128)(2,1)} %all-gather.10.cloned.1.call-done, bf16[2048,1408]{1,0:T(8,128)(2,1)} %all-gather.8.cloned.1.call-done, f32[256,1408]{1,0:T(8,128)} %fusion.46, bf16[256,2048]{1,0:T(8,128)(2,1)S(1)} %copy-done.2, bf16[256,2048]{1,0:T(8,128)(2,1)S(1)} %copy-done.1, ...), kind=kOutput, calls=%fused_computation.26 | convolution fusion | flops 2958622720 | bytes 16131072 | tf_op jit(solution)/shard_map/dot_general | solution.py:137
  415.9 32.7 %all-gather.12.cloned.1.call-done = bf16[1024,2048]{1,0:T(8,128)(2,1)} async-done(((bf16[256,2048]{1,0:T(8,128)(2,1)}), bf16[1024,2048]{1,0:T(8,128)(2,1)}) %all-gather.12.cloned.1.call-update) | async-done | bytes 4194320 | tf_op jit(solution)/shard_map/all_gather | solution.py:143
  448.6 4.2 reduce_sum.53
  452.9 2.7 add_convert_fusion
  (48 shorter events, 2.1 us)
Async XLA Ops:
  7.4 112.9 %copy-start = (bf16[256,2048]{1,0:T(8,128)(2,1)S(1)}, bf16[256,2048]{1,0:T(8,128)(2,1)}, u32[]{:S(2)}) copy-start(bf16[256,2048]{1,0:T(8,128)(2,1)} %param.23) | copy-start | bytes 3145732
  7.4 103.0 %copy-start.3 = (s32[256]{0:T(256)S(1)}, s32[256]{0:T(256)}, u32[]{:S(2)}) copy-start(s32[256]{0:T(256)} %param.20) | copy-start | bytes 3076
  7.4 155.8 %all-reduce.2.cloned.1.call-start = ((), (), s32[]{:S(2)}) async-start(), calls=%async_computation | async-start | bytes 2097152 | tf_op jit(solution)/shard_map/psum | solution.py:119
  120.1 43.0 %copy-start.1 = (bf16[256,2048]{1,0:T(8,128)(2,1)S(1)}, bf16[256,2048]{1,0:T(8,128)(2,1)}, u32[]{:S(2)}) copy-start(bf16[256,2048]{1,0:T(8,128)(2,1)} %param.16) | copy-start | bytes 3145732
  120.1 101.1 %copy-start.4 = (f32[2048]{0:T(1024)S(1)}, f32[2048]{0:T(1024)}, u32[]{:S(2)}) copy-start(f32[2048]{0:T(1024)} %param.24) | copy-start | bytes 24580
  121.7 99.5 %all-gather.6.cloned.1.call-start = ((), (), s32[]{:S(2)}) async-start(), calls=%async_computation.1 | async-start | bytes 6488064 | tf_op jit(solution)/shard_map/all_gather | solution.py:128
  122.3 191.9 %all-gather.10.cloned.1.call-start = ((), (), s32[]{:S(2)}) async-start(), calls=%async_computation.3 | async-start | bytes 6488064 | tf_op jit(solution)/shard_map/all_gather | solution.py:139
  122.9 283.7 %all-gather.8.cloned.1.call-start = ((), (), s32[]{:S(2)}) async-start(), calls=%async_computation.2 | async-start | bytes 6488064 | tf_op jit(solution)/shard_map/all_gather | solution.py:133
  123.5 325.1 %all-gather.12.cloned.1.call-start = ((), (), s32[]{:S(2)}) async-start(), calls=%async_computation.4 | async-start | bytes 5242880 | tf_op jit(solution)/shard_map/all_gather | solution.py:143
  164.8 241.8 %copy-start.2 = (bf16[256,2048]{1,0:T(8,128)(2,1)S(1)}, bf16[256,2048]{1,0:T(8,128)(2,1)}, u32[]{:S(2)}) copy-start(bf16[256,2048]{1,0:T(8,128)(2,1)} %all-reduce.2.cloned.1.call-done) | copy-start | bytes 3145732
Sparse Core Ops, SparseCore 0:
  121.9 41.2 all-reduce.1
  416.0 32.5 all-gather.11
Sparse Core Ops, SparseCore 1:
  124.4 96.8 all-gather.5
  223.1 91.0 all-gather.9
  316.3 90.3 all-gather.7
